TPU v7x, 32 devices: a whole 2x2x4 slice. The times are simulated.
32 devices in a mesh: fs: 8 (over z, x), tp: 4 (over y, core).
Axes of the slice: x: 2, y: 2, z: 4, core: 2. Of those that a mesh axis runs over, the one named last changes fastest.
Arguments:
- layer_inputs: bfloat16 [20480, 2048], P('fs'), may hold values from -6 to 6
- output_cot: bfloat16 [20480, 2048], P('fs'), may hold values from -6 to 6
- query_cot: bfloat16 [20480, 2048], P('fs', 'tp'), may hold values from -6 to 6
- head_outputs: bfloat16 [20480, 2048], P('fs', 'tp'), may hold values from -6 to 6
- weights: float32 [2, 2048, 2048], P(None, 'fs', 'tp'), may hold values from -0.125 to 0.125
- factors: bfloat16 [2, 2048, 256], replicated, may hold values from -0.125 to 0.125
- first_moment: float32 [2, 256, 2048], P(None, None, 'tp'), may hold values from -600 to 600
- second_moment: float32 [2, 256, 2048], P(None, None, 'tp'), may hold values from 1000 to 100000
Outputs:
- new_weights: float32 [2, 2048, 2048], P(None, 'fs', 'tp')
- update: float32 [2, 2048, 2048], P(None, 'fs', 'tp')
- new_first: float32 [2, 256, 2048], P(None, None, 'tp')
- new_second: float32 [2, 256, 2048], P(None, None, 'tp')
- weight_copy: bfloat16 [2, 2048, 2048], P(None, None, 'tp')
All inputs are finite; a program needn't handle non-finite values.
Results may differ from a plain program's by a relative error of at most 0.00055.
Values may be sent and summed in bfloat16 or wider, within the bound.
A program may use at most 128 MiB of HBM per device.

v0:
```python
from functools import partial

import jax
import jax.numpy as jnp
from jax import lax
from jax.sharding import PartitionSpec as P

D = 2048
QDIM = 2048


def block_terms(lefts, rights, projected, row_dev, extra, block, start, count):
    blocks = count // block
    pieces = []
    for index in range(len(lefts)):
        columns = lefts[index]
        grad = lax.dot_general(
            columns, rights[index], (((0,), (0,)), ((), ())), preferred_element_type=jnp.float32
        )
        pieces.append(grad.reshape(blocks, row_dev, -1))
    return jnp.concatenate(pieces, axis=1).reshape(count, -1)


def per_device(
    layer_inputs, output_cot, query_cot, head_outputs, weights, factors, first_moment, second_moment
):
    lefts = (layer_inputs, output_cot)
    rights = (query_cot, head_outputs)
    row_dev = weights.shape[1]
    position = lax.axis_index("fs")
    projected = (None, None)
    extra = 0
    block = 2 * (row_dev + extra)
    both = partial(block_terms, lefts, rights, projected, row_dev, extra, block)
    rows_all = lax.psum_scatter(
        both(jnp.int32(0), lax.axis_size("fs") * block), "fs", scatter_dimension=0, tiled=True
    ).reshape(2, row_dev + extra, -1)
    own_factors = lax.dynamic_slice_in_dim(factors, position * row_dev, row_dev, 1).astype(
        jnp.float32
    )
    partial_low = jnp.einsum("kdr,kdq->krq", own_factors, rows_all, precision=lax.Precision.HIGHEST)
    low = lax.psum(partial_low, "fs")
    first = 0.9 * first_moment + 0.1 * low
    second = 0.95 * second_moment + 0.05 * low * low
    normed = first / (jnp.sqrt(second) + 1e-06)
    sums = lax.psum(
        jnp.stack([jnp.sum(normed * normed, axis=(1, 2)), jnp.sum(low * low, axis=(1, 2))]), "tp"
    )
    ratio = jnp.sqrt(sums[0]) / jnp.sqrt(sums[1] + 1e-06)
    resid = rows_all - jnp.einsum("kdr,krq->kdq", own_factors, low, precision=lax.Precision.HIGHEST)
    step = (
        jnp.einsum("kdr,krq->kdq", own_factors, normed, precision=lax.Precision.HIGHEST)
        + ratio[:, None, None] * resid
    )
    total = lax.psum(jnp.sum(step * step), ("fs", "tp"))
    update = step * lax.rsqrt(total / (2.0 * D * QDIM) + 1e-06)
    new_weights = weights - 0.02 * update
    weight_copy = lax.all_gather(new_weights.astype(jnp.bfloat16), "fs", axis=1, tiled=True)
    return (new_weights, update, first, second, weight_copy)


def solution(mesh):
    return jax.shard_map(
        per_device,
        mesh=mesh,
        in_specs=(
            P("fs", None),
            P("fs", None),
            P("fs", "tp"),
            P("fs", "tp"),
            P(None, "fs", "tp"),
            P(),
            P(None, None, "tp"),
            P(None, None, "tp"),
        ),
        out_specs=(
            P(None, "fs", "tp"),
            P(None, "fs", "tp"),
            P(None, None, "tp"),
            P(None, None, "tp"),
            P(None, None, "tp"),
        ),
        check_vma=False,
    )
```

profile of v0, /device:TPU:16, one launch (start us, length us, event | category | flops | bytes accessed | tf_op | source)
XLA Modules:
  0.0 402.2 jit_solution(2077951097150191789)
XLA Ops:
  7.2 0.0 copy-start
  7.2 0.0 reduce-scatter.2.cloned.1.call-start
  7.2 1.7 copy-done
  8.9 0.0 copy-start.3
  8.9 0.0 copy-start.4
  8.9 8.5 %fusion.13 = f32[2048,512]{1,0:T(8,128)S(1)} fusion(bf16[2560,2048]{1,0:T(8,128)(2,1)} %param.8, bf16[2560,512]{1,0:T(8,128)(2,1)S(1)} %copy-done), kind=kOutput, calls=%fused_computation.24 | convolution fusion | flops 5368709120 | bytes 17301504 | tf_op jit(solution)/shard_map/dot_general | solution.py:17
  17.4 0.0 copy-done.3
  17.4 0.0 copy-done.4
  17.4 6.0 %fusion.14 = f32[2048,512]{1,0:T(8,128)S(1)} fusion(bf16[2560,2048]{1,0:T(8,128)(2,1)S(1)} %copy-done.3, bf16[2560,512]{1,0:T(8,128)(2,1)S(1)} %copy-done.4), kind=kOutput, calls=%fused_computation.25 | convolution fusion | flops 5368709120 | bytes 17301504 | tf_op jit(solution)/shard_map/dot_general | solution.py:17
  23.4 4.9 %pad_maximum_fusion = f32[8,512,512]{2,1,0:T(8,128)} fusion(f32[8,256,512]{2,1,0:T(8,128)S(1)} %bitcast.18, f32[8,256,512]{2,1,0:T(8,128)S(1)} %bitcast.17), kind=kLoop, calls=%fused_computation | loop fusion | flops 2097152 | bytes 16777216 | tf_op jit(solution)/shard_map/concatenate | solution.py:21
  28.3 0.0 reduce-scatter.2.cloned.1.call-update
  28.4 0.0 all-reduce.2.cloned.1.call-start
  28.4 147.7 %reduce-scatter.2.cloned.1.call-done = f32[512,512]{1,0:T(8,128)} async-done(((f32[4096,512]{1,0:T(8,128)}), f32[512,512]{1,0:T(8,128)}) %reduce-scatter.2.cloned.1.call-update) | async-done | bytes 1048592 | tf_op jit(solution)/shard_map/reduce_scatter | solution.py:35
  176.1 3.0 fusion.5
  179.1 0.0 all-reduce.2.cloned.1.call-update
  179.1 0.0 all-gather.2.cloned.1.call-start
  179.2 78.1 %all-reduce.2.cloned.1.call-done = f32[2,256,512]{2,1,0:T(8,128)} async-done(((f32[2,256,512]{2,1,0:T(8,128)}), f32[2,256,512]{2,1,0:T(8,128)}) %all-reduce.2.cloned.1.call-update) | async-done | bytes 1048592 | tf_op jit(solution)/shard_map/psum | solution.py:42
  257.3 3.9 multiply_reduce_fusion.2
  261.2 6.4 %psum.22 = f32[2,2]{1,0:T(2,128)S(1)} all-reduce(f32[2,2]{1,0:T(2,128)S(1)} %pad_maximum_fusion.1), channel_id=1, replica_groups=mesh['fs'=8,'tp'=4] {'tp'}, use_global_device_ids=true, to_apply=%region_4.0 | all-reduce | flops 4 | bytes 32 | tf_op jit(solution)/shard_map/psum | solution.py:46
  267.6 0.0 copy-start.1
  267.6 0.0 copy-start.2
  267.6 2.8 fusion.3
  270.4 0.0 copy-done.1
  270.5 0.0 copy-done.2
  270.5 3.3 multiply_reduce_fusion
  273.8 39.7 %psum.23 = f32[]{:T(128)} all-reduce(f32[]{:T(128)} %get-tuple-element.12), channel_id=1, replica_groups=mesh['fs'=8,'tp'=4] {'fs','tp'}, use_global_device_ids=true, to_apply=%region_6.0 | all-reduce | flops 1 | bytes 8 | tf_op jit(solution)/shard_map/psum | solution.py:55
  314.2 3.4 fusion.11
  317.6 0.0 all-gather.2.cloned.1.call-update
  317.6 73.5 %all-gather.2.cloned.1.call-done = bf16[2,2048,512]{2,1,0:T(8,128)(2,1)} async-done(((bf16[2,256,512]{2,1,0:T(8,128)(2,1)}), bf16[2,2048,512]{2,1,0:T(8,128)(2,1)}) %all-gather.2.cloned.1.call-update) | async-done | bytes 4194320 | tf_op jit(solution)/shard_map/all_gather | solution.py:58
  391.2 4.5 %copy.21 = bf16[2,2048,512]{2,1,0:T(8,128)(2,1)} copy(bf16[2,2048,512]{2,1,0:T(8,128)(2,1)} %all-gather.2.cloned.1.call-done) | data formatting | bytes 8388608
  (2 shorter events, 0.0 us)
Async XLA Ops:
  7.2 1.7 copy-start
  7.2 168.9 %reduce-scatter.2.cloned.1.call-start = ((), (), s32[]{:S(2)}) async-start(), calls=%async_computation.1 | async-start | bytes 9437184 | tf_op jit(solution)/shard_map/reduce_scatter | solution.py:35
  8.9 8.5 %copy-start.3 = (bf16[2560,2048]{1,0:T(8,128)(2,1)S(1)}, bf16[2560,2048]{1,0:T(8,128)(2,1)}, u32[]{:S(2)}) copy-start(bf16[2560,2048]{1,0:T(8,128)(2,1)} %param.9) | copy-start | bytes 31457284
  8.9 8.5 %copy-start.4 = (bf16[2560,512]{1,0:T(8,128)(2,1)S(1)}, bf16[2560,512]{1,0:T(8,128)(2,1)}, u32[]{:S(2)}) copy-start(bf16[2560,512]{1,0:T(8,128)(2,1)} %param.11) | copy-start | bytes 7864324
  28.4 228.9 %all-reduce.2.cloned.1.call-start = ((), (), s32[]{:S(2)}) async-start(), calls=%async_computation.2 | async-start | bytes 2097152 | tf_op jit(solution)/shard_map/psum | solution.py:42
  179.1 212.0 %all-gather.2.cloned.1.call-start = ((), (), s32[]{:S(2)}) async-start(), calls=%async_computation.3 | async-start | bytes 4718592 | tf_op jit(solution)/shard_map/all_gather | solution.py:58
  267.6 2.9 copy-start.1
  267.6 2.9 copy-start.2
Sparse Core Ops, SparseCore 0:
  28.5 147.6 reduce-scatter.1
  180.2 77.0 all-reduce.1
  317.8 73.3 all-gather.1
where the time goes:
time: 405 us; the launch traced here: 402 us
  waiting for transfers between devices  299 us (74%)
  blocking collectives  46.2 us (11%)
  matrix products  23.6 us (6%)
  between operations  14.5 us (4%)
  other arithmetic  12.2 us (3%)
  local copies, waits for them, and re-layouts  6.18 us (2%)
    reduce_scatter x1, waiting for transfers between devices, per_device(): lax.psum_scatter(both(jnp.int32(0), lax.axis_size('fs') * block), 'fs', s...  148 us
    psum x1, waiting for transfers between devices, per_device(): low = lax.psum(partial_low, 'fs')  78.1 us
    all_gather x1, waiting for transfers between devices, per_device(): lax.all_gather(new_weights.astype(jnp.bfloat16), 'fs', axis=1, tiled=True)  73.5 us
    psum x1, blocking collectives, per_device(): total = lax.psum(jnp.sum(step * step), ('fs', 'tp'))  39.7 us
    dot_general x2, matrix products, block_terms(): lax.dot_general(columns, rights[index], (((0,), (0,)), ((), ())), preferr...  14.5 us
  transfers between devices with their start and end apart: 3, of which 3 were waited for; matrix products, arithmetic and copies ran while one was open for 0% of the time, Pallas kernels for 0%

commit v1 on v0

v1 whole, which is shorter than its diff:
```python
from functools import partial

import jax
import jax.numpy as jnp
from jax import lax
from jax.experimental import pallas as pl
from jax.experimental.pallas import tpu as pltpu
from jax.sharding import PartitionSpec as P

MESH = pl.DeviceIdType.MESH
F32 = jnp.float32
BF16 = jnp.bfloat16


def dot(a, b):
    return lax.dot_general(a, b, (((1,), (0,)), ((), ())), preferred_element_type=F32)


def dot_t(a, b):
    return lax.dot_general(a, b, (((0,), (0,)), ((), ())), preferred_element_type=F32)


def split(value):
    high = value.astype(BF16)
    return high, (value - high.astype(F32)).astype(BF16)


def kernel(
    dims,
    x0, x1, y0, y1, w_in, f_in, m1_in, m2_in,
    o_w, o_u, o_first, o_second, o_copy,
    xv, yv, fv, wv, m1, m2,
    psend, pown, xrecv, zrecv,
    lpart, lxrecv, lsum, lzrecv, low, normed, step, gather,
    tpbuf, fsbuf, ttbuf,
    in_sem, out_sem, copy_sem,
    xs, xr, zs, zr, lxs, lxr, lzs, lzr, gzs, gzr, gxs, gxr, ts, tr, fss, fsr, tts, ttr, azs, azr, axs, axr,
):
    fs, tp, X, Z, H, lead = dims
    units = 2 * Z * H
    tokens, d = xv.shape[1], xv.shape[2]
    rows, cols = wv.shape[1], wv.shape[2]
    rank = fv.shape[2]
    half = cols // H
    rank_x, rank_f = rank // X, rank // fs
    me = lax.axis_index("fs")
    mt = lax.axis_index("tp")
    z, x = me // X, me % X

    def fs_at(jz, jx):
        return lax.rem(z + jz, Z) * X + lax.rem(x + jx, X)

    def remote(src, dst, ssem, rsem, fs_to=None, tp_to=None):
        dev = {"fs": fs_to} if tp_to is None else {"tp": tp_to}
        return pltpu.make_async_remote_copy(
            src_ref=src, dst_ref=dst, send_sem=ssem, recv_sem=rsem, device_id=dev, device_id_type=MESH
        )

    loads = [
        pltpu.make_async_copy(f_in, fv, in_sem.at[0]),
        pltpu.make_async_copy(x0, xv.at[0], in_sem.at[1]),
        pltpu.make_async_copy(y0, yv.at[0], in_sem.at[2]),
        pltpu.make_async_copy(x1, xv.at[1], in_sem.at[3]),
        pltpu.make_async_copy(y1, yv.at[1], in_sem.at[4]),
        pltpu.make_async_copy(m1_in, m1, in_sem.at[5]),
        pltpu.make_async_copy(m2_in, m2, in_sem.at[6]),
        pltpu.make_async_copy(w_in, wv, in_sem.at[7]),
    ]
    for load in loads:
        load.start()

    barrier = pltpu.get_barrier_semaphore()
    for j in range(1, fs):
        pl.semaphore_signal(barrier, inc=1, device_id={"fs": lax.rem(me + j, fs)}, device_id_type=MESH)
    for j in range(1, tp):
        pl.semaphore_signal(barrier, inc=1, device_id={"tp": lax.rem(mt + j, tp)}, device_id_type=MESH)
    pl.semaphore_wait(barrier, fs - 1 + tp - 1)

    chunk = tokens // 5 if tokens % 5 == 0 and (tokens // 5) % 128 == 0 else tokens
    loads[0].wait()
    for k in range(2):
        loads[1 + 2 * k].wait()
        loads[2 + 2 * k].wait()
        lpart[k] = jnp.zeros((rank, cols), F32)

        def project(c, carry, k=k):
            at = pl.ds(pl.multiple_of(c * chunk, 128), chunk)
            high, rest = split(dot(xv[k, at, :], fv[k]))
            right = yv[k, at, :]
            lpart[k] += dot_t(high, right) + dot_t(rest, right)
            return carry

        lax.fori_loop(0, tokens // chunk, project, 0)

    def low_x(j):
        to = lax.rem(x + j, X)
        at = pl.ds(pl.multiple_of(to * rank_x, 8), rank_x)
        return remote(lpart.at[:, at, :], lxrecv.at[j - 1], lxs.at[j - 1], lxr.at[j - 1], fs_to=fs_at(0, j))

    for j in range(1, X):
        low_x(j).start()

    def x_copy(u, j):
        return remote(
            psend.at[u, j - 1], xrecv.at[u, j - 1], xs.at[u, j - 1], xr.at[u, j - 1], fs_to=fs_at(0, j)
        )

    def unit(u):
        return lax.rem(u // (2 * H) + 1, Z), (u // H) % 2, u % H

    def grads(u, carry):
        jz, k, h = unit(u)
        right = yv[k, :, pl.ds(pl.multiple_of(h * half, 128), half)]

        def block(jx):
            at = pl.ds(pl.multiple_of(fs_at(jz, jx) * rows, 128), rows)
            return dot_t(xv[k, :, at], right)

        for j in range(1, X):
            psend[u, j - 1] = block(j)

        @pl.when(u < lead)
        def _():
            for j in range(1, X):
                x_copy(u, j).start()

        pown[u] = block(0)
        return carry

    first_part = units // 2
    lax.fori_loop(0, first_part, grads, 0)

    def low_z(j):
        at = pl.ds(pl.multiple_of(lax.rem(z + j, Z) * rank_f, 8), rank_f)
        return remote(lsum.at[:, at, :], lzrecv.at[j - 1], lzs.at[j - 1], lzr.at[j - 1], fs_to=fs_at(j, 0))

    for j in range(1, X):
        low_x(j).wait()
    total = lpart[:, pl.ds(pl.multiple_of(x * rank_x, 8), rank_x), :]
    for j in range(1, X):
        total = total + lxrecv[j - 1]
    lsum[...] = total
    for j in range(1, Z):
        low_z(j).start()

    lax.fori_loop(first_part, units, grads, 0)

    def gather_z(j, offset):
        block = low.at[x, lax.rem(z + offset, Z)]
        return remote(block, block, gzs.at[j - 1], gzr.at[j - 1], fs_to=fs_at(j, 0))

    def gather_x(j, offset):
        block = low.at[lax.rem(x + offset, X)]
        return remote(block, block, gxs.at[j - 1], gxr.at[j - 1], fs_to=fs_at(0, j))

    def tp_copy(j):
        return remote(tpbuf.at[0], tpbuf.at[j], ts.at[j - 1], tr.at[j - 1], tp_to=lax.rem(mt + j, tp))

    def z_copy(u):
        jz, k, h = unit(u)
        part = u % (2 * H)
        return remote(
            pown.at[u], zrecv.at[jz - 1, part], zs.at[jz - 1, part], zr.at[jz - 1, part], fs_to=fs_at(jz, 0)
        )

    def low_own():
        for j in range(1, Z):
            low_z(j).wait()
        value = lsum[:, pl.ds(pl.multiple_of(z * rank_f, 8), rank_f), :]
        for j in range(1, Z):
            value = value + lzrecv[j - 1]
        low[x, z] = value
        for j in range(1, Z):
            gather_z(j, 0).start()

    def low_row():
        for j in range(1, Z):
            gather_z(j, 0).wait_send()
            gather_z(j, Z - j).wait_recv()
        for j in range(1, X):
            gather_x(j, 0).start()

    def moments():
        for j in range(1, X):
            gather_x(j, 0).wait_send()
            gather_x(j, X - j).wait_recv()
        loads[5].wait()
        loads[6].wait()
        for k in range(2):
            nn = jnp.zeros((rank_f, cols), F32)
            ll = jnp.zeros((rank_f, cols), F32)
            for xi in range(X):
                for zi in range(Z):
                    at = slice((xi * Z + zi) * rank_f, (xi * Z + zi + 1) * rank_f)
                    value = low[xi, zi, k]
                    first = 0.9 * m1[k, at, :] + 0.1 * value
                    second = 0.95 * m2[k, at, :] + 0.05 * value * value
                    n = first / (jnp.sqrt(second) + 1e-06)
                    m1[k, at, :] = first
                    m2[k, at, :] = second
                    normed[k, at, :] = n
                    lpart[k, at, :] = value
                    nn = nn + n * n
                    ll = ll + value * value
            tpbuf[0, 2 * k] = jnp.full((8, 128), jnp.sum(nn), F32)
            tpbuf[0, 2 * k + 1] = jnp.full((8, 128), jnp.sum(ll), F32)
        pltpu.make_async_copy(m1, o_first, out_sem.at[0]).start()
        pltpu.make_async_copy(m2, o_second, out_sem.at[1]).start()
        for j in range(1, tp):
            tp_copy(j).start()

    ratio = [None, None]

    def project_back():
        for j in range(1, tp):
            tp_copy(j).wait()
        for k in range(2):
            nn, ll = tpbuf[0, 2 * k], tpbuf[0, 2 * k + 1]
            for j in range(1, tp):
                nn = nn + tpbuf[j, 2 * k]
                ll = ll + tpbuf[j, 2 * k + 1]
            ratio[k] = (jnp.sqrt(nn) / jnp.sqrt(ll + 1e-06))[0:1, 0:1]
            high, rest = split(normed[k] - ratio[k] * lpart[k])
            own = fv[k, pl.ds(pl.multiple_of(me * rows, 8), rows), :]
            step[k] = dot(own, high) + dot(own, rest)

    def at_unit(share):
        return min(units - 1, (units * share) // 16)

    todo = [(at_unit(2), low_own), (at_unit(6), low_row), (at_unit(11), moments), (at_unit(14), project_back)]
    for u in range(units):
        for j in range(1, X):
            x_copy(u, j).wait()
            if u + lead < units:
                x_copy(u + lead, j).start()
        value = pown[u]
        for j in range(1, X):
            value = value + xrecv[u, j - 1]
        pown[u] = value
        if u < units - 2 * H:
            z_copy(u).start()
        for when, job in todo:
            if when == u:
                job()

    squares = jnp.zeros((rows, half), F32)
    for part in range(2 * H):
        k, h = part // H, part % H
        value = pown[units - 2 * H + part]
        for j in range(1, Z):
            z_copy((j - 1) * 2 * H + part).wait()
            value = value + zrecv[j - 1, part]
        at = slice(h * half, (h + 1) * half)
        value = step[k, :, at] + ratio[k] * value
        step[k, :, at] = value
        squares = squares + value * value
    fsbuf[0] = jnp.full((8, 128), jnp.sum(squares), F32)

    def fs_copy(j):
        return remote(fsbuf.at[0], fsbuf.at[j], fss.at[j - 1], fsr.at[j - 1], fs_to=lax.rem(me + j, fs))

    def tt_copy(j):
        return remote(ttbuf.at[0], ttbuf.at[j], tts.at[j - 1], ttr.at[j - 1], tp_to=lax.rem(mt + j, tp))

    for j in range(1, fs):
        fs_copy(j).start()
    total = fsbuf[0]
    for j in range(1, fs):
        fs_copy(j).wait()
        total = total + fsbuf[j]
    ttbuf[0] = total
    for j in range(1, tp):
        tt_copy(j).start()
    for j in range(1, tp):
        tt_copy(j).wait()
        total = total + ttbuf[j]
    scale = lax.rsqrt(total / (2.0 * d * cols * tp) + 1e-06)[0:1, 0:1]

    def all_z(j, k, offset):
        block = gather.at[fs_at(offset, 0), k]
        return remote(block, block, azs.at[j - 1, k], azr.at[j - 1, k], fs_to=fs_at(j, 0))

    def all_x(s, j, k, zoff, xoff):
        block = gather.at[fs_at(zoff, xoff), k]
        return remote(block, block, axs.at[s, j - 1, k], axr.at[s, j - 1, k], fs_to=fs_at(0, j))

    def put(zoff, xoff, k):
        f = fs_at(zoff, xoff)
        at = pl.ds(pl.multiple_of(f * rows, 8), rows)
        return pltpu.make_async_copy(gather.at[f, k], o_copy.at[k, at, :], copy_sem.at[zoff, xoff, k])

    loads[7].wait()
    for k in range(2):
        update = step[k] * scale
        fresh = wv[k] - 0.02 * update
        gather[me, k] = fresh.astype(BF16)
        for j in range(1, Z):
            all_z(j, k, 0).start()
        for j in range(1, X):
            all_x(0, j, k, 0, 0).start()
        step[k] = update
        wv[k] = fresh
        put(0, 0, k).start()
    outs = [
        pltpu.make_async_copy(m1, o_first, out_sem.at[0]),
        pltpu.make_async_copy(m2, o_second, out_sem.at[1]),
        pltpu.make_async_copy(wv, o_w, out_sem.at[2]),
        pltpu.make_async_copy(step, o_u, out_sem.at[3]),
    ]
    outs[2].start()
    outs[3].start()
    for s in range(1, Z):
        for k in range(2):
            all_z(s, k, Z - s).wait_recv()
            for j in range(1, X):
                all_x(s, j, k, Z - s, 0).start()
            put(Z - s, 0, k).start()
    for s in range(Z):
        for k in range(2):
            for j in range(1, X):
                all_x(s, j, k, (Z - s) % Z, X - j).wait_recv()
                put((Z - s) % Z, X - j, k).start()
    for k in range(2):
        for s in range(1, Z):
            all_z(s, k, 0).wait_send()
        for s in range(Z):
            for j in range(1, X):
                all_x(s, j, k, (Z - s) % Z, 0).wait_send()
        for zo in range(Z):
            for xo in range(X):
                put(zo, xo, k).wait()
    for out in outs:
        out.wait()


def per_device(sizes, *args):
    layer_inputs, output_cot, query_cot, head_outputs, weights, factors, first_moment, second_moment = args
    fs, tp = sizes
    X = max(1, tp // 2)
    while fs % X:
        X -= 1
    Z = fs // X
    tokens, d = layer_inputs.shape
    rows, cols = weights.shape[1:]
    rank = factors.shape[2]
    H = 2 if cols % 256 == 0 else 1
    half = cols // H
    units = 2 * Z * H
    lead = min(3, units)
    vm, dma = pltpu.VMEM, pltpu.SemaphoreType.DMA
    x1, z1, t1, f1 = max(X - 1, 1), max(Z - 1, 1), max(tp - 1, 1), max(fs - 1, 1)
    scratch = [
        vm((2, tokens, d), BF16), vm((2, tokens, cols), BF16), vm((2, d, rank), BF16),
        vm((2, rows, cols), F32), vm((2, rank, cols), F32), vm((2, rank, cols), F32),
        vm((units, x1, rows, half), F32), vm((units, rows, half), F32), vm((units, x1, rows, half), F32),
        vm((z1, 2 * H, rows, half), F32),
        vm((2, rank, cols), F32), vm((x1, 2, rank // X, cols), F32), vm((2, rank // X, cols), F32),
        vm((z1, 2, rank // fs, cols), F32), vm((X, Z, 2, rank // fs, cols), F32),
        vm((2, rank, cols), F32), vm((2, rows, cols), F32), vm((fs, 2, rows, cols), BF16),
        vm((tp, 4, 8, 128), F32), vm((fs, 8, 128), F32), vm((tp, 8, 128), F32),
        dma((8,)), dma((4,)), dma((Z, X, 2)),
        dma((units, x1)), dma((units, x1)), dma((z1, 2 * H)), dma((z1, 2 * H)),
        dma((x1,)), dma((x1,)), dma((z1,)), dma((z1,)), dma((z1,)), dma((z1,)), dma((x1,)), dma((x1,)),
        dma((t1,)), dma((t1,)), dma((f1,)), dma((f1,)), dma((t1,)), dma((t1,)),
        dma((z1, 2)), dma((z1, 2)), dma((Z, x1, 2)), dma((Z, x1, 2)),
    ]
    anywhere = pl.BlockSpec(memory_space=pl.ANY)
    return tuple(pl.pallas_call(
        partial(kernel, (fs, tp, X, Z, H, lead)),
        out_shape=(
            jax.ShapeDtypeStruct(weights.shape, F32),
            jax.ShapeDtypeStruct(weights.shape, F32),
            jax.ShapeDtypeStruct(first_moment.shape, F32),
            jax.ShapeDtypeStruct(second_moment.shape, F32),
            jax.ShapeDtypeStruct((2, d, cols), BF16),
        ),
        in_specs=[anywhere] * 8,
        out_specs=(anywhere,) * 5,
        scratch_shapes=scratch,
        compiler_params=pltpu.CompilerParams(
            collective_id=0, has_side_effects=True, vmem_limit_bytes=67043328
        ),
    )(layer_inputs, output_cot, query_cot, head_outputs, weights, factors, first_moment, second_moment))


def solution(mesh):
    return jax.shard_map(
        partial(per_device, (mesh.shape["fs"], mesh.shape["tp"])),
        mesh=mesh,
        in_specs=(
            P("fs", None),
            P("fs", None),
            P("fs", "tp"),
            P("fs", "tp"),
            P(None, "fs", "tp"),
            P(),
            P(None, None, "tp"),
            P(None, None, "tp"),
        ),
        out_specs=(
            P(None, "fs", "tp"),
            P(None, "fs", "tp"),
            P(None, None, "tp"),
            P(None, None, "tp"),
            P(None, None, "tp"),
        ),
        check_vma=False,
    )
```

time: 405 us -> 244 us (0.60)
  waiting for transfers between devices: 299 us -> 0 us
  Pallas kernels: 0 us -> 235 us
  blocking collectives: 46.2 us -> 0 us
  matrix products: 23.6 us -> 0 us
  between operations: 14.5 us -> 0.67 us
  other arithmetic: 12.2 us -> 0 us
    pallas_call x0 -> x1, Pallas kernels: none -> 235 us  [per_device(): pl.pallas_call(partial(kernel, (fs, tp, X, Z, H, lead)), out_shape=(jax.S...]
    reduce_scatter x1 -> x0, waiting for transfers between devices: 148 us -> none  [per_device(): lax.psum_scatter(both(jnp.int32(0), lax.axis_size('fs') * block), 'fs', s...]
    psum x1 -> x0, waiting for transfers between devices: 78.1 us -> none  [per_device(): low = lax.psum(partial_low, 'fs')]
    all_gather x1 -> x0, waiting for transfers between devices: 73.5 us -> none  [per_device(): lax.all_gather(new_weights.astype(jnp.bfloat16), 'fs', axis=1, tiled=True)]
    psum x2 -> x0, blocking collectives: 46.2 us -> none  [the longest x1 39.7 us: per_device(): total = lax.psum(jnp.sum(step * step), ('fs', 'tp'))]
    dot_general x5 -> x0, matrix products: 23.6 us -> none  [the longest x2 14.5 us: block_terms(): lax.dot_general(columns, rights[index], (((0,), (0,)), ((), ())), preferr...]
    concatenate x1 -> x0, other arithmetic: 4.92 us -> none  [block_terms(): return jnp.concatenate(pieces, axis=1).reshape(count, -1)]
  transfers between devices with their start and end apart: 3 -> 0, of which waited for: 3 -> 0; matrix products, arithmetic and copies ran while one was open for 0% -> 0% of each run, Pallas kernels for 0% -> 0%
where the time goes in v1:
time: 244 us
  Pallas kernels  235 us (96%)
  local copies, waits for them, and re-layouts  8.73 us (4%)
    pallas_call x1, Pallas kernels, per_device(): pl.pallas_call(partial(kernel, (fs, tp, X, Z, H, lead)), out_shape=(jax.S...  235 us
    unnamed x11, local copies, waits for them, and re-layouts  8.73 us

profile of v1, /device:TPU:16, one launch (start us, length us, event | category | flops | bytes accessed | tf_op | source)
XLA Modules:
  0.0 244.0 jit_solution(13051098004083517913)
XLA Ops:
  0.6 234.6 %shard_map.119 = (f32[2,256,512]{2,1,0:T(8,128)}, f32[2,256,512]{2,1,0:T(8,128)}, f32[2,256,512]{2,1,0:T(8,128)}, f32[2,256,512]{2,1,0:T(8,128)}, bf16[2,2048,512]{2,1,0:T(8,128)(2,1)}) custom-call(bf16[2560,2048]{1,0:T(8,128)(2,1)} %x0.1, bf16[2560,2048]{1,0:T(8,128)(2,1)} %x1.1, bf16[2560,512]{1,0:T(8,128)(2,1)} %y0.1, bf16[2560,512]{1,0:T(8,128)(2,1)} %y1.1, ...), custom_call_target="tpu_custom_call" | custom-call | tf_op jit(solution)/shard_map/pallas_call | solution.py:368
  235.2 0.0 copy-start.2
  235.2 0.0 copy-start.1
  235.3 0.0 copy-start
  235.3 2.4 copy.18
  237.7 2.4 copy.19
  240.0 0.0 copy-done.2
  240.0 1.0 copy.20
  241.0 0.0 copy-done.1
  241.0 1.0 copy.21
  242.0 0.0 copy-done
  242.0 2.0 copy.22
Async XLA Ops:
  235.2 4.8 %copy-start.2 = (f32[2,256,512]{2,1,0:T(8,128)S(1)}, f32[2,256,512]{2,1,0:T(8,128)}, u32[]{:S(2)}) copy-start(f32[2,256,512]{2,1,0:T(8,128)} %get-tuple-element.12) | copy-start | bytes 3145732
  235.2 5.8 %copy-start.1 = (f32[2,256,512]{2,1,0:T(8,128)S(1)}, f32[2,256,512]{2,1,0:T(8,128)}, u32[]{:S(2)}) copy-start(f32[2,256,512]{2,1,0:T(8,128)} %get-tuple-element.13) | copy-start | bytes 3145732
  235.3 6.7 %copy-start = (bf16[2,2048,512]{2,1,0:T(8,128)(2,1)S(1)}, bf16[2,2048,512]{2,1,0:T(8,128)(2,1)}, u32[]{:S(2)}) copy-start(bf16[2,2048,512]{2,1,0:T(8,128)(2,1)} %get-tuple-element.14) | copy-start | bytes 12582916
